TPU v7x, 32 devices: a whole 2x2x4 slice. The times are simulated.
32 devices in a mesh: sp: 8 (over z, x), tp: 4 (over y, core).
Axes of the slice: x: 2, y: 2, z: 4, core: 2. Of those that a mesh axis runs over, the one named last changes fastest.
Arguments:
- residual_matrix: bfloat16 [2048, 2048], P(('sp', 'tp')), may hold values from -6 to 6
- query_vectors: bfloat16 [2048, 2048], P('tp', 'sp'), may hold values from -6 to 6
- lookup_vectors: bfloat16 [2048, 2048], P('tp', 'sp'), may hold values from -6 to 6
- payload_vectors: bfloat16 [2048, 2048], P('tp', 'sp'), may hold values from -6 to 6
- fading_dependent_term: bfloat16 [2048, 2048], P('tp', 'sp'), may hold values from -4 to 4
- step_size_preactivation: bfloat16 [2048, 2048], P('tp', 'sp'), may hold values from -8 to 8
- attention_result_switch: bfloat16 [2048, 2048], P('tp', 'sp'), may hold values from -6 to 6
- fading_bias_vector: float32 [2048], P('tp'), may hold values from -16 to -2
- surplus_forgetting: float32 [32, 2048], P('tp', 'sp'), may hold values from -0.7 to 0
- per_group_scaler: float32 [2048], P('tp'), may hold values from 0.1 to 1.9
- attention_result_matrix: bfloat16 [2048, 2048], P('tp'), may hold values from -0.125 to 0.125
- dense_block_scaler: float32 [2048], replicated, may hold values from 0.1 to 1.9
- switching_matrix: bfloat16 [2048, 5632], P('sp', 'tp'), may hold values from -0.125 to 0.125
- expanding_matrix: bfloat16 [2048, 5632], P('sp', 'tp'), may hold values from -0.125 to 0.125
- contracting_matrix: bfloat16 [5632, 2048], P('tp', 'sp'), may hold values from -0.078125 to 0.078125
Outputs:
- blended: bfloat16 [2048, 2048], P(('sp', 'tp'))
All inputs are finite; a program needn't handle non-finite values.
Results may differ from a plain program's by a relative error of at most 0.015.
Values may be sent and summed in bfloat16 or wider, within the bound.
A program may use at most 128 MiB of HBM per device.

v0:
```python
import jax
import jax.numpy as jnp
from jax import lax
from jax.sharding import PartitionSpec as P

HEAD = 64
BLOCK = 64
norm_eps = 1e-06
group_eps = 0.00064
key_eps = 1e-06
highest = lax.Precision.HIGHEST


def carried_in(x, axis, join, neutral):
    place = lax.axis_index(axis)
    gathered = jax.tree.map(
        lambda a, kind: lax.all_gather(a.astype(kind), axis),
        x,
        jax.tree.map(lambda a: jnp.bfloat16 if a.dtype == jnp.float32 else a.dtype, x),
    )
    state = jax.tree.map(lambda a, e: jnp.zeros_like(a) + jnp.asarray(e, a.dtype), x, neutral)

    def one(turn, state):
        return join(
            state,
            jax.tree.map(
                lambda a, own: lax.dynamic_index_in_dim(a, turn, 0, False).astype(own.dtype),
                gathered,
                x,
            ),
        )

    return lax.fori_loop(0, place, one, state)


def by_blocks(source, attention_group_count, position_count):
    return (
        source.astype(jnp.float32)
        .reshape(attention_group_count, HEAD, position_count // BLOCK, BLOCK)
        .transpose(0, 2, 3, 1)
    )


def compose(earlier, latter):
    return (
        jnp.einsum("...ij,...jk->...ik", earlier[0], latter[0], precision=highest),
        jnp.einsum("...ij,...jk->...ik", earlier[1], latter[0], precision=highest) + latter[1],
    )


def unit_lower_solve(mutual, right_side):
    power = -mutual
    solved = right_side
    for level in range((BLOCK - 1).bit_length()):
        solved = solved + jnp.einsum("hbts,hbsn->hbtn", power, solved, precision=highest)
        if level + 1 < (BLOCK - 1).bit_length():
            power = jnp.einsum("hbts,hbsu->hbtu", power, power, precision=highest)
    return solved


def rms_rows(middle, dense_block_scaler):
    scale_rows = lax.rsqrt(jnp.mean(middle * middle, axis=-1, keepdims=True) + norm_eps)
    return (middle * scale_rows * dense_block_scaler).astype(jnp.bfloat16)


def local(
    residual_matrix,
    query_vectors,
    lookup_vectors,
    payload_vectors,
    fading_dependent_term,
    step_size_preactivation,
    attention_result_switch,
    fading_bias_vector,
    surplus_forgetting,
    per_group_scaler,
    attention_result_matrix,
    dense_block_scaler,
    switching_matrix,
    expanding_matrix,
    contracting_matrix,
):
    attention_group_count = surplus_forgetting.shape[0]
    position_count = surplus_forgetting.shape[1]
    block_count = position_count // BLOCK
    read_rows = by_blocks(query_vectors, attention_group_count, position_count)
    key_rows = by_blocks(lookup_vectors, attention_group_count, position_count)
    value_rows = by_blocks(payload_vectors, attention_group_count, position_count)
    fading_preactivation = by_blocks(
        fading_dependent_term, attention_group_count, position_count
    ) + fading_bias_vector.reshape(attention_group_count, 1, 1, HEAD)
    log_fading_factor = -jnp.exp(
        -jax.nn.softplus(-fading_preactivation) - 0.5
    ) + surplus_forgetting.reshape(attention_group_count, block_count, BLOCK, 1)
    learn_rate = jax.nn.sigmoid(
        by_blocks(step_size_preactivation, attention_group_count, position_count)
    )
    unit_keys = key_rows * lax.rsqrt(jnp.sum(key_rows * key_rows, axis=-1, keepdims=True) + key_eps)
    scaled = key_rows * learn_rate
    removal = unit_keys * learn_rate
    cum_after = jnp.cumsum(log_fading_factor, axis=2)
    before = cum_after - log_fading_factor
    cum_final = cum_after[:, :, -1:, :]
    probe_keys = unit_keys * jnp.exp(before)
    removal_in = removal * jnp.exp(-cum_after)
    scaled_in = scaled * jnp.exp(-cum_after)
    reads_out = read_rows * jnp.exp(cum_after)
    position = jnp.arange(BLOCK)
    strict = position[:, None] > position[None, :]
    up_to = position[:, None] >= position[None, :]
    mutual = jnp.where(
        strict, jnp.einsum("hbtn,hbsn->hbts", probe_keys, removal_in, precision=highest), 0.0
    )
    through = jnp.where(
        strict, jnp.einsum("hbtn,hbsn->hbts", probe_keys, scaled_in, precision=highest), 0.0
    )
    right_side = jnp.concatenate(
        [probe_keys, jnp.einsum("hbts,hbsn->hbtn", through, value_rows, precision=highest)], axis=-1
    )
    solved = unit_lower_solve(mutual, right_side)
    basis_part = solved[..., :HEAD]
    offset = solved[..., HEAD:]
    removal_end = removal * jnp.exp(cum_final - cum_after)
    scaled_end = scaled * jnp.exp(cum_final - cum_after)
    carry_map = jnp.eye(HEAD, dtype=jnp.float32) * jnp.exp(cum_final) - jnp.einsum(
        "hbtk,hbtj->hbkj", basis_part, removal_end, precision=highest
    )
    carry_add = jnp.einsum(
        "hbtv,hbtj->hbvj", value_rows, scaled_end, precision=highest
    ) - jnp.einsum("hbtv,hbtj->hbvj", offset, removal_end, precision=highest)
    block_maps = (jnp.moveaxis(carry_map, 1, 0), jnp.moveaxis(carry_add, 1, 0))
    identity = (
        jnp.broadcast_to(jnp.eye(HEAD, dtype=jnp.float32), (attention_group_count, HEAD, HEAD)),
        jnp.zeros((attention_group_count, HEAD, HEAD), jnp.float32),
    )

    def fold_step(total_map, member):
        return (compose(total_map, member), None)

    summary, _ = lax.scan(fold_step, identity, block_maps)
    _, entering = carried_in(summary, "sp", compose, identity)

    def walk_step(carried, member):
        moved_on = jnp.einsum("hvk,hkj->hvj", carried, member[0], precision=highest) + member[1]
        return (moved_on, carried)

    _, starts = lax.scan(walk_step, entering, block_maps)
    starts = jnp.moveaxis(starts, 0, 1)
    removed = -jnp.einsum("hbtk,hbvk->hbtv", basis_part, starts, precision=highest) - offset
    reach_removal = jnp.where(
        up_to, jnp.einsum("hbtn,hbsn->hbts", reads_out, removal_in, precision=highest), 0.0
    )
    reach_value = jnp.where(
        up_to, jnp.einsum("hbtn,hbsn->hbts", reads_out, scaled_in, precision=highest), 0.0
    )
    outputs = (
        jnp.einsum("hbtk,hbvk->hbtv", reads_out, starts, precision=highest)
        + jnp.einsum("hbts,hbsv->hbtv", reach_removal, removed, precision=highest)
        + jnp.einsum("hbts,hbsv->hbtv", reach_value, value_rows, precision=highest)
    )
    centred = outputs - jnp.mean(outputs, axis=-1, keepdims=True)
    normed_heads = centred * lax.rsqrt(
        jnp.mean(centred * centred, axis=-1, keepdims=True) + group_eps
    )
    normed_heads = normed_heads.transpose(0, 3, 1, 2).reshape(
        attention_group_count * HEAD, position_count
    )
    mixed_out = (
        normed_heads * per_group_scaler[:, None] * attention_result_switch.astype(jnp.float32)
    ).astype(jnp.bfloat16)
    moved_rows = lax.all_to_all(mixed_out, "tp", split_axis=1, concat_axis=0, tiled=True)
    whole_weight = lax.all_gather(attention_result_matrix, "tp", axis=0, tiled=True)
    middle = residual_matrix.astype(jnp.float32) + jnp.einsum(
        "ct,cd->td", moved_rows, whole_weight, preferred_element_type=jnp.float32
    )
    normed = rms_rows(middle, dense_block_scaler)
    all_rows = lax.all_gather(normed, "tp", axis=0, tiled=True)
    gate_sum = jnp.dot(
        all_rows,
        lax.all_gather(switching_matrix, "sp", axis=0, tiled=True),
        preferred_element_type=jnp.float32,
    )
    up_sum = jnp.dot(
        all_rows,
        lax.all_gather(expanding_matrix, "sp", axis=0, tiled=True),
        preferred_element_type=jnp.float32,
    )
    hidden = (jax.nn.silu(gate_sum) * up_sum).astype(jnp.bfloat16)
    down_full = lax.all_gather(contracting_matrix, "sp", axis=1, tiled=True)
    channel_out = lax.psum_scatter(
        jnp.dot(hidden, down_full, preferred_element_type=jnp.float32).astype(jnp.bfloat16),
        "tp",
        scatter_dimension=0,
        tiled=True,
    ).astype(jnp.float32)
    return (middle + channel_out).astype(jnp.bfloat16)


def solution(mesh):
    placed = (
        P(("sp", "tp"), None),
        P("tp", "sp"),
        P("tp", "sp"),
        P("tp", "sp"),
        P("tp", "sp"),
        P("tp", "sp"),
        P("tp", "sp"),
        P("tp"),
        P("tp", "sp"),
        P("tp"),
        P("tp", None),
        P(),
        P("sp", "tp"),
        P("sp", "tp"),
        P("tp", "sp"),
    )
    return jax.shard_map(
        local, mesh=mesh, in_specs=placed, out_specs=P(("sp", "tp"), None), check_vma=False
    )
```

profile of v0, /device:TPU:0, one launch (start us, length us, event | category | flops | bytes accessed | tf_op | source)
XLA Modules:
  0.0 466.2 jit_solution(5035272207007485328)
XLA Ops:
  8.1 1.4 reshape.86
  12.3 1.7 bitcast_multiply_fusion.4
  16.3 1.5 reshape.88
  17.8 1.7 copy.92
  19.5 3.8 fusion.46
  23.4 3.4 convolution_select_fusion.3
  26.8 2.8 fusion.23
  30.7 2.7 convolution_bitcast_fusion.6
  33.4 2.3 fusion.55
  36.9 1.4 convolution_add_fusion.6
  39.5 1.2 convolution_add_fusion.5
  40.8 1.6 fusion.69
  42.4 1.2 convolution_add_fusion.4
  44.8 1.2 convolution_add_fusion.3
  47.2 1.2 convolution_add_fusion.2
  50.6 2.1 fusion.21
  53.9 4.5 fusion.22
  58.4 2.5 copy.103
  61.0 17.9 %while.39 = (s32[]{:T(128)}, f32[8,64,64]{1,2,0:T(8,128)S(1)}, f32[8,64,64]{1,2,0:T(8,128)}, f32[4,8,64,64]{2,3,1,0:T(8,128)}, f32[4,8,64,64]{2,3,1,0:T(8,128)}, /*index=5*/s32[]{:T(128)}, s32[]{:T(128)}) while((s32[]{:T(128)}, f32[8,64,64]{1,2,0:T(8,128)S(1)}, f32[8,64,64]{1,2,0:T(8,128)}, f32[4,8,64,64]{2,3,1,0:T(8,128)}, ...), condition=%wide.region_3.4_spmd.clone, body=%wide.region_2.3_spmd.clone.sunk | while | flops 50397184 | bytes 1836631 | solution.py:140
  62.0 2.1 fusion.137
  64.1 1.3 convolution_bitcast_fusion.8
  66.4 2.1 fusion.137
  68.6 1.4 convolution_bitcast_fusion.8
  70.9 2.1 fusion.137
  73.0 1.3 convolution_bitcast_fusion.8
  75.4 2.1 fusion.137
  77.5 1.3 convolution_bitcast_fusion.8
  80.1 40.5 %all-gather = bf16[64,64,64]{2,1,0:T(8,128)(2,1)} all-gather(bf16[8,64,64]{2,1,0:T(8,128)(2,1)S(1)} %copy.105), channel_id=2, replica_groups=mesh['sp'=8,'tp'=4] {'sp'}, dimensions={0}, use_global_device_ids=true | all-gather | bytes 589824 | tf_op jit(solution)/shard_map/all_gather | solution.py:17
  120.7 39.5 %all-gather.1 = bf16[64,64,64]{2,1,0:T(8,128)(2,1)} all-gather(bf16[8,64,64]{2,1,0:T(8,128)(2,1)S(1)} %copy.106), channel_id=3, replica_groups=mesh['sp'=8,'tp'=4] {'sp'}, dimensions={0}, use_global_device_ids=true | all-gather | bytes 589824 | tf_op jit(solution)/shard_map/all_gather | solution.py:17
  160.1 8.8 %while.38 = (s32[]{:T(128)}, f32[8,64,64]{1,2,0:T(8,128)S(1)}, f32[4,8,64,64]{2,3,1,0:T(8,128)}, f32[4,8,64,64]{2,3,1,0:T(8,128)}, f32[4,8,64,64]{2,3,1,0:T(8,128)}, /*index=5*/s32[]{:T(128)}) while((s32[]{:T(128)}, f32[8,64,64]{1,2,0:T(8,128)S(1)}, f32[4,8,64,64]{2,3,1,0:T(8,128)}, f32[4,8,64,64]{2,3,1,0:T(8,128)}, ...), condition=%wide.region_7.8_spmd, body=%wide.region_6.7_spmd.sunk | while | flops 25198592 | bytes 1443397 | solution.py:147
  160.9 1.4 fusion.132
  163.1 1.4 fusion.132
  165.3 1.4 fusion.132
  167.5 1.4 fusion.132
  169.0 3.3 fusion.20
  172.2 3.9 fusion.44
  176.2 2.3 convolution_select_fusion.1
  178.5 1.9 convolution_add_fusion.8
  180.5 3.2 convolution_select_fusion
  186.2 8.6 %all_to_all.19 = bf16[512,4,64]{0,2,1:T(8,128)(2,1)S(1)} all-to-all(bf16[512,4,64]{0,2,1:T(8,128)(2,1)S(1)} %bitcast.213), channel_id=1, replica_groups=mesh['sp'=8,'tp'=4] {'tp'}, dimensions={1} | all-to-all | bytes 524288 | tf_op jit(solution)/shard_map/all_to_all | solution.py:171
  194.9 5.1 %multiply_reduce_fusion.1 = (f32[64]{0:T(128)S(1)}, f32[64,2048]{1,0:T(8,128)S(1)}) fusion(bf16[2048,64]{0,1:T(8,128)(2,1)S(1)} %bitcast.211, bf16[2048,2048]{1,0:T(8,128)(2,1)} %all-gather.8.cloned.1.call-done, bf16[64,2048]{1,0:T(8,128)(2,1)S(1)} %copy-done.10), kind=kOutput, calls=%fused_computation.97 | convolution fusion | flops 537395136 | bytes 9437440 | tf_op jit(solution)/shard_map/ct,cd->td/dot_general | solution.py:173
  202.0 35.8 %all-gather.10.cloned.1.call-done = bf16[256,2048]{1,0:T(8,128)(2,1)} async-done(((bf16[64,2048]{1,0:T(8,128)(2,1)}), bf16[256,2048]{1,0:T(8,128)(2,1)}) %all-gather.10.cloned.1.call-update) | async-done | bytes 1048592 | tf_op jit(solution)/shard_map/all_gather | solution.py:177
  237.8 4.8 %fusion.72 = f32[256,1408]{1,0:T(8,128)S(1)} fusion(bf16[256,2048]{1,0:T(8,128)(2,1)} %all-gather.10.cloned.1.call-done, bf16[2048,1408]{1,0:T(8,128)(2,1)} %all-gather.12.cloned.1.call-done), kind=kOutput, calls=%fused_computation.122 | convolution fusion | flops 1476395008 | bytes 8257536 | tf_op jit(solution)/shard_map/dot_general | solution.py:178
  242.7 89.5 %all-gather.14.cloned.1.call-done = bf16[2048,1408]{1,0:T(8,128)(2,1)} async-done(((bf16[256,1408]{1,0:T(8,128)(2,1)}), bf16[2048,1408]{1,0:T(8,128)(2,1)}) %all-gather.14.cloned.1.call-update) | async-done | bytes 5767184 | tf_op jit(solution)/shard_map/all_gather | solution.py:185
  332.2 93.2 %all-gather.16.cloned.1.call-done = bf16[1408,2048]{1,0:T(8,128)(2,1)} async-done(((bf16[1408,256]{1,0:T(8,128)(2,1)}), bf16[1408,2048]{1,0:T(8,128)(2,1)}) %all-gather.16.cloned.1.call-update) | async-done | bytes 5767184 | tf_op jit(solution)/shard_map/all_gather | solution.py:189
  425.4 8.8 %convolution_convert_fusion = bf16[256,2048]{1,0:T(8,128)(2,1)} fusion(bf16[1408,2048]{1,0:T(8,128)(2,1)} %all-gather.16.cloned.1.call-done, bf16[256,2048]{1,0:T(8,128)(2,1)S(1)} %copy-done.19, bf16[2048,1408]{1,0:T(8,128)(2,1)} %all-gather.14.cloned.1.call-done, f32[256,1408]{1,0:T(8,128)S(1)} %fusion.72), kind=kOutput, calls=%fused_computation.28 | convolution fusion | flops 2955476992 | bytes 15073280 | tf_op jit(solution)/shard_map/dot_general | solution.py:191
  434.3 23.1 %reduce-scatter.2.cloned.1.call-done = bf16[64,2048]{1,0:T(8,128)(2,1)} async-done(((bf16[256,2048]{1,0:T(8,128)(2,1)}), bf16[64,2048]{1,0:T(8,128)(2,1)}) %reduce-scatter.2.cloned.1.call-update) | async-done | bytes 262160 | tf_op jit(solution)/shard_map/reduce_scatter | solution.py:190
  457.4 1.7 add_convert_fusion
  (114 shorter events, 28.5 us)
Async XLA Ops:
  6.5 3.3 copy-start.16
  6.5 3.4 copy-start.18
  6.5 3.5 copy-start.11
  6.5 188.3 %all-gather.8.cloned.1.call-start = ((), (), s32[]{:S(2)}) async-start(), calls=%async_computation.2 | async-start | bytes 10485760 | tf_op jit(solution)/shard_map/all_gather | solution.py:172
  7.3 194.8 %all-gather.12.cloned.1.call-start = ((), (), s32[]{:S(2)}) async-start(), calls=%async_computation.4 | async-start | bytes 6488064 | tf_op jit(solution)/shard_map/all_gather | solution.py:180
  8.0 229.8 %all-gather.10.cloned.1.call-start = ((), (), s32[]{:S(2)}) async-start(), calls=%async_computation.3 | async-start | bytes 1310720 | tf_op jit(solution)/shard_map/all_gather | solution.py:177
  9.5 4.5 copy-start.12
  9.9 1.6 copy-start.8
  23.3 3.5 copy-start.2
  23.3 3.5 copy-start.5
  23.4 6.2 %copy-start.13 = (bf16[512,256]{1,0:T(8,128)(2,1)S(1)}, bf16[512,256]{1,0:T(8,128)(2,1)}, u32[]{:S(2)}) copy-start(bf16[512,256]{1,0:T(8,128)(2,1)} %param.24) | copy-start | bytes 786436
  30.7 5.1 %copy-start.4 = (f32[8,4,64,64]{3,2,1,0:T(8,128)S(1)}, f32[8,4,64,64]{3,2,1,0:T(8,128)}, u32[]{:S(2)}) copy-start(f32[8,4,64,64]{3,2,1,0:T(8,128)} %fusion.23) | copy-start | bytes 1572868
  30.7 6.3 %copy-start.3 = (f32[8,4,64,64]{3,2,1,0:T(8,128)S(1)}, f32[8,4,64,64]{3,2,1,0:T(8,128)}, u32[]{:S(2)}) copy-start(f32[8,4,64,64]{3,2,1,0:T(8,128)} %copy-done.2) | copy-start | bytes 1572868
  44.8 5.8 %copy-start.7 = (f32[8,4,64,64]{3,2,1,0:T(8,128)S(1)}, f32[8,4,64,64]{3,2,1,0:T(8,128)}, u32[]{:S(2)}) copy-start(f32[8,4,64,64]{3,2,1,0:T(8,128)} %get-tuple-element.192) | copy-start | bytes 1572868
  49.6 1.0 copy-start.1
  169.0 7.2 %copy-start = (f32[8,4,64,64]{3,0,1,2:T(8,128)S(1)}, f32[8,4,64,64]{3,0,1,2:T(8,128)}, u32[]{:S(2)}) copy-start(f32[8,4,64,64]{3,0,1,2:T(8,128)} %get-tuple-element.196) | copy-start | bytes 1572868
  169.0 7.2 %copy-start.6 = (f32[8,4,64,64]{3,2,1,0:T(8,128)S(1)}, f32[8,4,64,64]{3,2,1,0:T(8,128)}, u32[]{:S(2)}) copy-start(f32[8,4,64,64]{3,2,1,0:T(8,128)} %copy-done.5) | copy-start | bytes 1572868
  176.2 7.5 %copy-start.9 = (bf16[8,64,4,64]{3,2,1,0:T(4,128)(2,1)S(1)}, bf16[8,64,4,64]{3,2,1,0:T(4,128)(2,1)}, u32[]{:S(2)}) copy-start(bf16[8,64,4,64]{3,2,1,0:T(4,128)(2,1)} %reshape.74) | copy-start | bytes 786436
  183.7 2.3 copy-start.14
  183.7 2.5 copy-start.17
  183.7 11.2 %copy-start.10 = (bf16[64,2048]{1,0:T(8,128)(2,1)S(1)}, bf16[64,2048]{1,0:T(8,128)(2,1)}, u32[]{:S(2)}) copy-start(bf16[64,2048]{1,0:T(8,128)(2,1)} %param.21) | copy-start | bytes 786436
  194.8 5.1 %copy-start.15 = (f32[2048]{0:T(1024)S(1)}, f32[2048]{0:T(1024)}, u32[]{:S(2)}) copy-start(f32[2048]{0:T(1024)} %param.32) | copy-start | bytes 24580
  200.8 131.4 %all-gather.14.cloned.1.call-start = ((), (), s32[]{:S(2)}) async-start(), calls=%async_computation.5 | async-start | bytes 6488064 | tf_op jit(solution)/shard_map/all_gather | solution.py:185
  201.4 224.0 %all-gather.16.cloned.1.call-start = ((), (), s32[]{:S(2)}) async-start(), calls=%async_computation.6 | async-start | bytes 6488064 | tf_op jit(solution)/shard_map/all_gather | solution.py:189
  202.0 255.4 %reduce-scatter.2.cloned.1.call-start = ((), (), s32[]{:S(2)}) async-start(), calls=%async_computation.7 | async-start | bytes 1310720 | tf_op jit(solution)/shard_map/reduce_scatter | solution.py:190
  237.8 187.6 %copy-start.19 = (bf16[256,2048]{1,0:T(8,128)(2,1)S(1)}, bf16[256,2048]{1,0:T(8,128)(2,1)}, u32[]{:S(2)}) copy-start(bf16[256,2048]{1,0:T(8,128)(2,1)} %all-gather.10.cloned.1.call-done) | copy-start | bytes 3145732
Sparse Core Ops, SparseCore 0:
  8.9 60.9 all-gather.7
  72.1 118.7 all-gather.11
  200.9 36.8 all-gather.9
  239.9 92.2 all-gather.13
  334.1 91.2 all-gather.15
  434.4 22.9 reduce-scatter.1
where the time goes:
time: 472 us; the launch traced here: 466 us
  waiting for transfers between devices  244 us (52%)
  blocking collectives  88.6 us (19%)
  matrix products  85.6 us (18%)
  local copies, waits for them, and re-layouts  22.1 us (5%)
  between operations  14.3 us (3%)
  other arithmetic  11.1 us (2%)
    all_gather x1, waiting for transfers between devices, local(): down_full = lax.all_gather(contracting_matrix, 'sp', axis=1, tiled=True)  93.2 us
    all_gather x1, waiting for transfers between devices, local(): lax.all_gather(expanding_matrix, 'sp', axis=0, tiled=True)  89.5 us
    all_gather x2, blocking collectives, carried_in(): lax.all_gather(a.astype(kind), axis)  80 us
    all_gather x1, waiting for transfers between devices, local(): all_rows = lax.all_gather(normed, 'tp', axis=0, tiled=True)  35.8 us
    reduce_scatter x1, waiting for transfers between devices, local(): lax.psum_scatter(jnp.dot(hidden, down_full, preferred_element_type=jnp.fl...  23.1 us
  transfers between devices with their start and end apart: 6, of which 4 were waited for; matrix products, arithmetic and copies ran while one was open for 23% of the time, Pallas kernels for 0%

commit v1 on v0

--- a/solution.py
+++ b/solution.py
@@ -186,7 +186,7 @@
         preferred_element_type=jnp.float32,
     )
     hidden = (jax.nn.silu(gate_sum) * up_sum).astype(jnp.bfloat16)
-    down_full = lax.all_gather(contracting_matrix, "sp", axis=1, tiled=True)
+    down_full = jnp.concatenate(lax.all_gather(contracting_matrix, "sp"), axis=1)
     channel_out = lax.psum_scatter(
         jnp.dot(hidden, down_full, preferred_element_type=jnp.float32).astype(jnp.bfloat16),
         "tp",

time: 472 us -> 443 us (0.939)
  waiting for transfers between devices: 244 us -> 206 us
  local copies, waits for them, and re-layouts: 22.1 us -> 30.5 us
    all_gather x1, waiting for transfers between devices: 93.2 us -> 0.02 us  [local(): lax.all_gather(contracting_matrix, 'sp')]
    all_gather x1, waiting for transfers between devices: 0.02 us -> 74.3 us  [local(): lax.all_gather(switching_matrix, 'sp', axis=0, tiled=True)]
    all_gather x1, waiting for transfers between devices: 35.8 us -> 16.3 us  [local(): all_rows = lax.all_gather(normed, 'tp', axis=0, tiled=True)]
    reshape x0 -> x1, local copies, waits for them, and re-layouts: none -> 8.32 us  [local(): jnp.concatenate(lax.all_gather(contracting_matrix, 'sp'), axis=1)]
  transfers between devices with their start and end apart: 6 -> 6, of which waited for: 4 -> 4; matrix products, arithmetic and copies ran while one was open for 23% -> 27% of each run, Pallas kernels for 0% -> 0%
where the time goes in v1:
time: 443 us; the launch traced here: 436 us
  waiting for transfers between devices  206 us (47%)
  blocking collectives  88.1 us (20%)
  matrix products  85.7 us (19%)
  local copies, waits for them, and re-layouts  30.5 us (7%)
  between operations  14.3 us (3%)
  other arithmetic  11 us (2%)
    all_gather x1, waiting for transfers between devices, local(): lax.all_gather(expanding_matrix, 'sp', axis=0, tiled=True)  89.5 us
    all_gather x2, blocking collectives, carried_in(): lax.all_gather(a.astype(kind), axis)  79.6 us
    all_gather x1, waiting for transfers between devices, local(): lax.all_gather(switching_matrix, 'sp', axis=0, tiled=True)  74.3 us
    reduce_scatter x1, waiting for transfers between devices, local(): lax.psum_scatter(jnp.dot(hidden, down_full, preferred_element_type=jnp.fl...  23.2 us
    all_gather x1, waiting for transfers between devices, local(): all_rows = lax.all_gather(normed, 'tp', axis=0, tiled=True)  16.3 us
  transfers between devices with their start and end apart: 6, of which 4 were waited for; matrix products, arithmetic and copies ran while one was open for 27% of the time, Pallas kernels for 0%

profile of v1, /device:TPU:0, one launch (start us, length us, event | category | flops | bytes accessed | tf_op | source)
XLA Modules:
  0.0 436.1 jit_solution(14488553108037863280)
XLA Ops:
  8.8 1.4 reshape.95
  13.0 1.7 bitcast_multiply_fusion.4
  17.0 1.5 reshape.97
  18.5 1.7 copy.132
  20.2 3.8 fusion.46
  24.1 3.5 convolution_select_fusion.3
  27.5 2.9 fusion.23
  31.5 2.7 convolution_bitcast_fusion.6
  34.2 2.3 fusion.55
  37.7 1.4 convolution_add_fusion.6
  40.3 1.2 convolution_add_fusion.5
  41.6 1.6 fusion.69
  45.6 1.2 convolution_add_fusion.3
  51.4 2.1 fusion.21
  53.5 1.2 copy.144
  54.8 4.5 %fusion.22 = f32[4,8,64,64]{3,2,0,1:T(8,128)} fusion(f32[8,4,64,64]{3,2,1,0:T(8,128)} %get-tuple-element.202, f32[8,4,64,128]{3,2,1,0:T(8,128)} %copy-done.1, f32[4,8,64]{2,0,1:T(4,128)S(1)} %copy.127, f32[64,64]{1,0:T(8,128)S(1)} %fusion.61), kind=kOutput, calls=%fused_computation.43 | convolution fusion | flops 100925440 | bytes 2121728 | tf_op jit(solution)/shard_map/hbtk,hbtj->hbkj/dot_general | solution.py:125
  59.4 2.6 copy.143
  62.0 17.9 %while.39 = (s32[]{:T(128)}, f32[8,64,64]{1,2,0:T(8,128)S(1)}, f32[8,64,64]{1,2,0:T(8,128)}, f32[4,8,64,64]{2,3,1,0:T(8,128)}, f32[4,8,64,64]{2,3,1,0:T(8,128)}, /*index=5*/s32[]{:T(128)}, s32[]{:T(128)}) while((s32[]{:T(128)}, f32[8,64,64]{1,2,0:T(8,128)S(1)}, f32[8,64,64]{1,2,0:T(8,128)}, f32[4,8,64,64]{2,3,1,0:T(8,128)}, ...), condition=%wide.region_3.4_spmd.clone, body=%wide.region_2.3_spmd.clone.sunk | while | flops 50397184 | bytes 1836631 | solution.py:140
  63.0 2.1 fusion.137
  65.1 1.3 convolution_bitcast_fusion.8
  67.4 2.1 fusion.137
  69.6 1.3 convolution_bitcast_fusion.8
  71.9 2.1 fusion.137
  74.0 1.3 convolution_bitcast_fusion.8
  76.4 2.1 fusion.137
  78.5 1.4 convolution_bitcast_fusion.8
  81.1 40.1 %all-gather = bf16[64,64,64]{2,1,0:T(8,128)(2,1)} all-gather(bf16[8,64,64]{2,1,0:T(8,128)(2,1)S(1)} %copy.145), channel_id=2, replica_groups=mesh['sp'=8,'tp'=4] {'sp'}, dimensions={0}, use_global_device_ids=true | all-gather | bytes 589824 | tf_op jit(solution)/shard_map/all_gather | solution.py:17
  121.3 39.5 %all-gather.1 = bf16[64,64,64]{2,1,0:T(8,128)(2,1)} all-gather(bf16[8,64,64]{2,1,0:T(8,128)(2,1)S(1)} %copy.146), channel_id=3, replica_groups=mesh['sp'=8,'tp'=4] {'sp'}, dimensions={0}, use_global_device_ids=true | all-gather | bytes 589824 | tf_op jit(solution)/shard_map/all_gather | solution.py:17
  160.8 8.8 %while.38 = (s32[]{:T(128)}, f32[8,64,64]{1,2,0:T(8,128)S(1)}, f32[4,8,64,64]{2,3,1,0:T(8,128)}, f32[4,8,64,64]{2,3,1,0:T(8,128)}, f32[4,8,64,64]{2,3,1,0:T(8,128)}, /*index=5*/s32[]{:T(128)}) while((s32[]{:T(128)}, f32[8,64,64]{1,2,0:T(8,128)S(1)}, f32[4,8,64,64]{2,3,1,0:T(8,128)}, f32[4,8,64,64]{2,3,1,0:T(8,128)}, ...), condition=%wide.region_7.8_spmd, body=%wide.region_6.7_spmd.sunk | while | flops 25198592 | bytes 1443397 | solution.py:147
  161.6 1.4 fusion.132
  163.8 1.4 fusion.132
  166.0 1.4 fusion.132
  168.1 1.4 fusion.132
  169.6 3.3 fusion.20
  172.9 3.9 fusion.44
  176.8 2.3 convolution_select_fusion.1
  179.2 1.9 convolution_add_fusion.8
  181.1 3.2 convolution_select_fusion
  186.9 8.4 %all_to_all.19 = bf16[512,4,64]{0,2,1:T(8,128)(2,1)S(1)} all-to-all(bf16[512,4,64]{0,2,1:T(8,128)(2,1)S(1)} %bitcast.219), channel_id=1, replica_groups=mesh['sp'=8,'tp'=4] {'tp'}, dimensions={1} | all-to-all | bytes 524288 | tf_op jit(solution)/shard_map/all_to_all | solution.py:171
  195.4 5.1 %multiply_reduce_fusion.1 = (f32[64]{0:T(128)S(1)}, f32[64,2048]{1,0:T(8,128)S(1)}) fusion(bf16[2048,64]{0,1:T(8,128)(2,1)S(1)} %bitcast.217, bf16[2048,2048]{1,0:T(8,128)(2,1)} %all-gather.9.cloned.1.call-done, bf16[64,2048]{1,0:T(8,128)(2,1)S(1)} %copy-done.10), kind=kOutput, calls=%fused_computation.97 | convolution fusion | flops 537395136 | bytes 9437440 | tf_op jit(solution)/shard_map/ct,cd->td/dot_general | solution.py:173
  202.0 8.3 %copy.160 = bf16[1408,8,256]{0,2,1:T(8,128)(2,1)} copy(bf16[1408,8,256]{2,0,1:T(8,128)(2,1)} %bitcast.213) | data formatting | bytes 11534336 | tf_op jit(solution)/shard_map/reshape | solution.py:189
  210.3 74.3 %all-gather.13.cloned.1.call-done = bf16[2048,1408]{1,0:T(8,128)(2,1)} async-done(((bf16[256,1408]{1,0:T(8,128)(2,1)}), bf16[2048,1408]{1,0:T(8,128)(2,1)}) %all-gather.13.cloned.1.call-update) | async-done | bytes 5767184 | tf_op jit(solution)/shard_map/all_gather | solution.py:180
  284.6 16.3 %all-gather.11.cloned.1.call-done = bf16[256,2048]{1,0:T(8,128)(2,1)} async-done(((bf16[64,2048]{1,0:T(8,128)(2,1)}), bf16[256,2048]{1,0:T(8,128)(2,1)}) %all-gather.11.cloned.1.call-update) | async-done | bytes 1048592 | tf_op jit(solution)/shard_map/all_gather | solution.py:177
  301.0 4.8 %fusion.72 = f32[256,1408]{1,0:T(8,128)S(1)} fusion(bf16[256,2048]{1,0:T(8,128)(2,1)} %all-gather.11.cloned.1.call-done, bf16[2048,1408]{1,0:T(8,128)(2,1)} %all-gather.13.cloned.1.call-done), kind=kOutput, calls=%fused_computation.122 | convolution fusion | flops 1476395008 | bytes 8257536 | tf_op jit(solution)/shard_map/dot_general | solution.py:178
  305.8 89.5 %all-gather.15.cloned.1.call-done = bf16[2048,1408]{1,0:T(8,128)(2,1)} async-done(((bf16[256,1408]{1,0:T(8,128)(2,1)}), bf16[2048,1408]{1,0:T(8,128)(2,1)}) %all-gather.15.cloned.1.call-update) | async-done | bytes 5767184 | tf_op jit(solution)/shard_map/all_gather | solution.py:185
  395.3 8.8 %convolution_convert_fusion = bf16[256,2048]{1,0:T(8,128)(2,1)} fusion(bf16[1408,2048]{0,1:T(8,128)(2,1)} %bitcast.214, bf16[256,2048]{1,0:T(8,128)(2,1)S(1)} %copy-done.19, bf16[2048,1408]{1,0:T(8,128)(2,1)} %all-gather.15.cloned.1.call-done, f32[256,1408]{1,0:T(8,128)S(1)} %fusion.72), kind=kOutput, calls=%fused_computation.28 | convolution fusion | flops 2955476992 | bytes 15073280 | tf_op jit(solution)/shard_map/dot_general | solution.py:191
  404.2 23.2 %reduce-scatter.2.cloned.1.call-done = bf16[64,2048]{1,0:T(8,128)(2,1)} async-done(((bf16[256,2048]{1,0:T(8,128)(2,1)}), bf16[64,2048]{1,0:T(8,128)(2,1)}) %reduce-scatter.2.cloned.1.call-update) | async-done | bytes 262160 | tf_op jit(solution)/shard_map/reduce_scatter | solution.py:190
  427.3 1.7 add_convert_fusion
  (115 shorter events, 29.9 us)
Async XLA Ops:
  6.5 4.1 copy-start.16
  6.5 4.2 copy-start.18
  6.5 4.2 copy-start.11
  6.5 188.8 %all-gather.9.cloned.1.call-start = ((), (), s32[]{:S(2)}) async-start(), calls=%async_computation.2 | async-start | bytes 10485760 | tf_op jit(solution)/shard_map/all_gather | solution.py:172
  7.3 194.7 %all-gather.17.cloned.1.call-start = ((), (), s32[]{:S(2)}) async-start(), calls=%async_computation.7 | async-start | bytes 6488064 | tf_op jit(solution)/shard_map/all_gather | solution.py:189
  8.0 276.6 %all-gather.13.cloned.1.call-start = ((), (), s32[]{:S(2)}) async-start(), calls=%async_computation.4 | async-start | bytes 6488064 | tf_op jit(solution)/shard_map/all_gather | solution.py:180
  8.7 292.2 %all-gather.11.cloned.1.call-start = ((), (), s32[]{:S(2)}) async-start(), calls=%async_computation.3 | async-start | bytes 1310720 | tf_op jit(solution)/shard_map/all_gather | solution.py:177
  10.3 4.5 %copy-start.12 = (bf16[512,256]{1,0:T(8,128)(2,1)S(1)}, bf16[512,256]{1,0:T(8,128)(2,1)}, u32[]{:S(2)}) copy-start(bf16[512,256]{1,0:T(8,128)(2,1)} %param.23) | copy-start | bytes 786436
  10.6 1.6 copy-start.8
  24.0 3.5 copy-start.2
  24.0 3.5 copy-start.5
  24.0 6.4 %copy-start.13 = (bf16[512,256]{1,0:T(8,128)(2,1)S(1)}, bf16[512,256]{1,0:T(8,128)(2,1)}, u32[]{:S(2)}) copy-start(bf16[512,256]{1,0:T(8,128)(2,1)} %param.24) | copy-start | bytes 786436
  31.5 5.1 %copy-start.4 = (f32[8,4,64,64]{3,2,1,0:T(8,128)S(1)}, f32[8,4,64,64]{3,2,1,0:T(8,128)}, u32[]{:S(2)}) copy-start(f32[8,4,64,64]{3,2,1,0:T(8,128)} %fusion.23) | copy-start | bytes 1572868
  31.5 6.3 %copy-start.3 = (f32[8,4,64,64]{3,2,1,0:T(8,128)S(1)}, f32[8,4,64,64]{3,2,1,0:T(8,128)}, u32[]{:S(2)}) copy-start(f32[8,4,64,64]{3,2,1,0:T(8,128)} %copy-done.2) | copy-start | bytes 1572868
  45.6 5.8 %copy-start.7 = (f32[8,4,64,64]{3,2,1,0:T(8,128)S(1)}, f32[8,4,64,64]{3,2,1,0:T(8,128)}, u32[]{:S(2)}) copy-start(f32[8,4,64,64]{3,2,1,0:T(8,128)} %get-tuple-element.202) | copy-start | bytes 1572868
  50.4 1.0 copy-start.1
  169.6 7.2 %copy-start = (f32[8,4,64,64]{3,0,1,2:T(8,128)S(1)}, f32[8,4,64,64]{3,0,1,2:T(8,128)}, u32[]{:S(2)}) copy-start(f32[8,4,64,64]{3,0,1,2:T(8,128)} %get-tuple-element.206) | copy-start | bytes 1572868
  169.6 7.2 %copy-start.6 = (f32[8,4,64,64]{3,2,1,0:T(8,128)S(1)}, f32[8,4,64,64]{3,2,1,0:T(8,128)}, u32[]{:S(2)}) copy-start(f32[8,4,64,64]{3,2,1,0:T(8,128)} %copy-done.5) | copy-start | bytes 1572868
  176.8 7.5 %copy-start.9 = (bf16[8,64,4,64]{3,2,1,0:T(4,128)(2,1)S(1)}, bf16[8,64,4,64]{3,2,1,0:T(4,128)(2,1)}, u32[]{:S(2)}) copy-start(bf16[8,64,4,64]{3,2,1,0:T(4,128)(2,1)} %reshape.80) | copy-start | bytes 786436
  184.3 2.4 copy-start.14
  184.3 2.5 copy-start.17
  184.3 11.0 %copy-start.10 = (bf16[64,2048]{1,0:T(8,128)(2,1)S(1)}, bf16[64,2048]{1,0:T(8,128)(2,1)}, u32[]{:S(2)}) copy-start(bf16[64,2048]{1,0:T(8,128)(2,1)} %param.21) | copy-start | bytes 786436
  195.3 5.1 %copy-start.15 = (f32[2048]{0:T(1024)S(1)}, f32[2048]{0:T(1024)}, u32[]{:S(2)}) copy-start(f32[2048]{0:T(1024)} %param.32) | copy-start | bytes 24580
  201.3 194.0 %all-gather.15.cloned.1.call-start = ((), (), s32[]{:S(2)}) async-start(), calls=%async_computation.5 | async-start | bytes 6488064 | tf_op jit(solution)/shard_map/all_gather | solution.py:185
  201.9 225.4 %reduce-scatter.2.cloned.1.call-start = ((), (), s32[]{:S(2)}) async-start(), calls=%async_computation.6 | async-start | bytes 1310720 | tf_op jit(solution)/shard_map/reduce_scatter | solution.py:190
  301.0 94.4 %copy-start.19 = (bf16[256,2048]{1,0:T(8,128)(2,1)S(1)}, bf16[256,2048]{1,0:T(8,128)(2,1)}, u32[]{:S(2)}) copy-start(bf16[256,2048]{1,0:T(8,128)(2,1)} %all-gather.11.cloned.1.call-done) | copy-start | bytes 3145732
Sparse Core Ops, SparseCore 0:
  8.9 60.9 all-gather.8
  72.1 119.2 all-gather.16
  193.6 90.9 all-gather.12
  286.0 14.8 all-gather.10
  303.0 92.2 all-gather.14
  404.3 22.9 reduce-scatter.1
